TPU v7x, 32 devices: a whole 2x2x4 slice. The times are simulated.
32 devices in a mesh: sp: 8 (over z, x), dp: 4 (over y, core).
Axes of the slice: x: 2, y: 2, z: 4, core: 2. Of those that a mesh axis runs over, the one named last changes fastest.
Arguments:
- queries: bfloat16 [4, 1024, 2048], P('dp', 'sp'), may hold values from -12 to 12
- key_rows: bfloat16 [4, 1024, 2048], P('dp', 'sp'), may hold values from -12 to 12
- value_rows: bfloat16 [4, 1024, 2048], P('dp', 'sp'), may hold values from -6 to 6
- lambdas: float32 [16], P('sp'), may hold values from 0.3 to 0.8
- head_gain: float32 [128], replicated, may hold values from 0.1 to 1.9
- out_weight: bfloat16 [2048, 2048], replicated, may hold values from -0.125 to 0.125
- residual: bfloat16 [4, 1024, 2048], P('dp', 'sp'), may hold values from -6 to 6
- mixer_gain: float32 [2048], replicated, may hold values from 0.1 to 1.9
- channel_gain: float32 [2048], replicated, may hold values from 0.1 to 1.9
- expert_gain: float32 [2048], replicated, may hold values from 0.1 to 1.9
- routes: int32 [4, 1024, 2], P('dp', 'sp'), may hold values from 0 to 7, all different within a row; in each aligned block of 128 rows (0 to 127, 128 to 255, ..., all dimensions but the last counted through in order) at most 48 rows name the same one
- route_logits: float32 [4, 1024, 2], P('dp', 'sp'), may hold values from -5 to 5
- gate_weight: bfloat16 [8, 2048, 4096], P('sp', None, 'dp'), may hold values from -0.125 to 0.125
- up_weight: bfloat16 [8, 2048, 4096], P('sp', None, 'dp'), may hold values from -0.125 to 0.125
- down_weight: bfloat16 [8, 4096, 2048], P('sp', 'dp'), may hold values from -0.09375 to 0.09375
Outputs:
- updated: bfloat16 [4, 1024, 2048], P('dp', 'sp')
Inputs may be any that keep to these rules, and one draw needn't show every extreme that they name: `routes`: among the rows of one device no expert is named by more than 48 rows; in some of these blocks one expert is named by exactly 48.
All inputs are finite; a program needn't handle non-finite values.
Results may differ from a plain program's by a relative error of at most 0.014.
Values may be sent and summed in bfloat16 or wider, within the bound.
A program may use at most 128 MiB of HBM per device.

v0:
```python
import functools
import math

import jax
import jax.numpy as jnp
from jax import lax
from jax.experimental import pallas as pl
from jax.experimental.pallas import tpu as pltpu
from jax.sharding import PartitionSpec as P


MESH = pl.DeviceIdType.MESH


def rms_scale(values, epsilon):
    return values * lax.rsqrt(jnp.mean(values * values, axis=-1, keepdims=True) + epsilon)


def attention_kernel(
    count,
    heads,
    query_ref,
    key_ref,
    value_ref,
    cos_ref,
    sin_ref,
    lambda_ref,
    head_gain_ref,
    residual_ref,
    mixer_gain_ref,
    channel_gain_ref,
    routes_ref,
    logits_ref,
    weight_hbm,
    stream_ref,
    normed_ref,
    place_ref,
    mix_ref,
    query_out,
    key_out,
    query_in,
    key_in,
    value_in,
    head_out,
    token_rows,
    projected,
    weight,
    w_sem,
    in_send,
    in_recv,
    out_send,
    out_recv,
):
    me = lax.axis_index("sp")
    tokens, model = query_ref.shape
    lanes = head_gain_ref.shape[1]
    map_dim = lanes // 2
    scale = map_dim ** (-0.5)
    load = pltpu.make_async_copy(weight_hbm, weight, w_sem)
    load.start()

    def sp_at(step):
        return {"sp": (me + step + count) % count}

    def columns(owner, h):
        return pl.ds(pl.multiple_of((owner * heads + h) * lanes, lanes), lanes)

    def far(k):
        return count // 2 + (k // 2) * (2 * (k % 2) - 1)

    def dest_columns(k, h):
        return columns((me + far(k)) % count, h)

    def remote(src, dst, send, recv, step):
        return pltpu.make_async_remote_copy(
            src_ref=src,
            dst_ref=dst,
            send_sem=send,
            recv_sem=recv,
            device_id=sp_at(step),
            device_id_type=MESH,
        )

    def inward(h, k, i):
        sources = (value_ref.at[:, dest_columns(k, h)], query_out.at[h, k], key_out.at[h, k])
        targets = (value_in.at[h, k], query_in.at[h, k], key_in.at[h, k])
        return remote(sources[i], targets[i], in_send.at[h, i, k], in_recv.at[h, i, k], far(k))

    def outward(h, k):
        return remote(
            head_out.at[h, k], token_rows.at[:, columns(me, h)], out_send.at[h, k], out_recv.at[h, k], -far(k)
        )

    barrier = pltpu.get_barrier_semaphore()
    for k in range(1, count):
        pl.semaphore_signal(barrier, inc=1, device_id=sp_at(k), device_id_type=MESH)

    first_half = lax.broadcasted_iota(jnp.int32, (tokens, lanes), 1) % map_dim < map_dim // 2

    def turned(ref, cols):
        x = ref[:, cols].astype(jnp.float32)
        ahead = pltpu.roll(x, lanes - map_dim // 2, 1)
        behind = pltpu.roll(x, map_dim // 2, 1)
        return x * cos_ref[...] + jnp.where(first_half, ahead, behind) * sin_ref[...]

    def prepare(h, cols):
        query = (turned(query_ref, cols) * scale).astype(jnp.bfloat16)
        key = turned(key_ref, cols).astype(jnp.bfloat16)
        return query, key

    for h in range(heads):
        query, key = prepare(h, columns(me, h))
        query_in[h, 0] = query
        key_in[h, 0] = key
        value_in[h, 0] = value_ref[:, columns(me, h)]

    pl.semaphore_wait(barrier, count - 1)

    for h in range(heads):

        @pl.loop(1, count)
        def _(k):
            inward(h, k, 0).start()

        @pl.loop(1, count)
        def _(k):
            query_out[h, k], key_out[h, k] = prepare(h, dest_columns(k, h))

        @pl.loop(1, count)
        def _(k):
            inward(h, k, 1).start()
            inward(h, k, 2).start()

    top = routes_ref.shape[1]
    capacity = mix_ref.shape[1] // count
    experts = lax.broadcasted_iota(jnp.int32, (tokens, 128), 1)
    places = lax.broadcasted_iota(jnp.int32, mix_ref.shape, 1)
    lower = lax.broadcasted_iota(jnp.int32, (tokens, tokens), 0)
    lower = (lower >= lax.broadcasted_iota(jnp.int32, (tokens, tokens), 1)).astype(jnp.bfloat16)
    logits = logits_ref[...]
    odds = jnp.exp(logits - jnp.max(logits, axis=-1, keepdims=True))
    shares = odds / jnp.sum(odds, axis=-1, keepdims=True)
    used = jnp.zeros((1, 128), jnp.float32)
    mix = jnp.zeros(mix_ref.shape, jnp.float32)
    place = jnp.zeros(mix_ref.shape, jnp.float32)
    for i in range(top):
        away = routes_ref[:, i : i + 1] - me
        away = jnp.where(away < 0, away + count, away)
        mid = count // 2
        ranked = jnp.where(away < mid, 2 * (mid - away), 2 * (away - mid) + 1)
        ranked = jnp.where(away == 0, 0, ranked)
        named = (experts == ranked).astype(jnp.float32)
        running = jnp.dot(lower, named.astype(jnp.bfloat16), preferred_element_type=jnp.float32)
        slot = jnp.sum(named * (running + used), axis=-1, keepdims=True).astype(jnp.int32) - 1
        used = used + jnp.sum(named, axis=0, keepdims=True)
        hit = places == ranked * capacity + slot
        mix = mix + jnp.where(hit, shares[:, i : i + 1], 0.0)
        place = place + jnp.where(hit, 1.0, 0.0)
    mix_ref[...] = mix
    place_ref[...] = place.astype(jnp.bfloat16)

    width = 2
    rows = width * tokens
    length = count * tokens
    in_first = lax.broadcasted_iota(jnp.int32, (rows, lanes), 1) < map_dim

    def part_of(total):
        return jnp.exp(total - jnp.max(total, axis=-1, keepdims=True))

    for h in range(heads):

        @pl.loop(1, count)
        def _(k):
            for i in range(3):
                inward(h, k, i).wait_recv()

        @pl.loop(0, count // width)
        def _(b):
            query = query_in[h, pl.ds(b * width, width)].reshape(rows, lanes).astype(jnp.float32)
            both = jnp.concatenate(
                [jnp.where(in_first, query, 0.0), jnp.where(in_first, 0.0, query)], axis=0
            ).astype(jnp.bfloat16)
            keys = key_in[h].reshape(length, lanes)
            scores = lax.dot_general(
                both, keys, (((1,), (1,)), ((), ())), preferred_element_type=jnp.float32
            )
            one, two = part_of(scores[:rows]), part_of(scores[rows:])
            one_scale = 1.0 / jnp.sum(one, axis=-1, keepdims=True)
            two_scale = lambda_ref[h] / jnp.sum(two, axis=-1, keepdims=True)
            mixing = (one * one_scale - two * two_scale).astype(jnp.bfloat16)
            mix = jnp.dot(
                mixing, value_in[h].reshape(length, lanes), preferred_element_type=jnp.float32
            )
            result = (rms_scale(mix, 1e-05) * head_gain_ref[...]).astype(jnp.bfloat16)
            head_out[h, pl.ds(b * width, width)] = result.reshape(width, tokens, lanes)
            for i in range(width):
                k = b * width + i

                @pl.when(k > 0)
                def _():
                    outward(h, k).start()

    for h in range(heads):
        token_rows[:, columns(me, h)] = head_out[h, 0]

    load.wait()
    for h in range(heads):

        @pl.loop(1, count)
        def _(k):
            outward(h, k).wait_recv()

    wide = math.gcd(model, 512)

    @pl.loop(0, model // wide)
    def _(n):
        cols = pl.ds(pl.multiple_of(n * wide, wide), wide)
        projected[:, cols] = jnp.dot(
            token_rows[...], weight[:, cols], preferred_element_type=jnp.float32
        )

    chunk = math.gcd(tokens, 16)

    @pl.loop(0, tokens // chunk)
    def _(n):
        part = pl.ds(pl.multiple_of(n * chunk, chunk), chunk)
        stream = residual_ref[part, :].astype(jnp.float32)
        stream = stream + rms_scale(projected[part, :], 1e-06) * mixer_gain_ref[...]
        stream = stream.astype(jnp.bfloat16)
        stream_ref[part, :] = stream
        normed = rms_scale(stream.astype(jnp.float32), 1e-06) * channel_gain_ref[...]
        normed_ref[part, :] = normed.astype(jnp.bfloat16)

    for h in range(heads):

        @pl.loop(1, count)
        def _(k):
            for i in range(3):
                inward(h, k, i).wait_send()
            outward(h, k).wait_send()


def attention_stage(
    queries,
    keys,
    values,
    lambdas,
    head_gain,
    out_weight,
    residual,
    mixer_gain,
    channel_gain,
    routes,
    logits,
):
    count = lax.axis_size("sp")
    heads = lambdas.shape[0]
    lanes = head_gain.shape[0]
    map_dim = lanes // 2
    tokens, model = residual.shape
    inverse = 1.0 / 10000.0 ** (jnp.arange(0, map_dim, 2, dtype=jnp.float32) / map_dim)
    positions = lax.axis_index("sp") * tokens + jnp.arange(tokens, dtype=jnp.int32)
    angles = positions.astype(jnp.float32)[:, None] * inverse[None, :]
    cosine, sine = jnp.cos(angles), jnp.sin(angles)
    cos_table = jnp.concatenate([cosine] * 4, axis=1)
    sin_table = jnp.concatenate([-sine, sine] * 2, axis=1)
    vmem = pl.BlockSpec(memory_space=pltpu.VMEM)
    smem = pl.BlockSpec(memory_space=pltpu.SMEM)
    half = jnp.bfloat16
    dma = pltpu.SemaphoreType.DMA
    blocks = pltpu.VMEM((heads, count, tokens, lanes), half)
    shape = jax.ShapeDtypeStruct((tokens, model), half)
    capacity = -(-max(2, 3 * tokens // count) // 16) * 16
    table = (tokens, count * capacity)
    return pl.pallas_call(
        functools.partial(attention_kernel, count, heads),
        out_shape=[
            shape,
            shape,
            jax.ShapeDtypeStruct(table, half),
            jax.ShapeDtypeStruct(table, jnp.float32),
        ],
        in_specs=[vmem] * 5 + [smem] + [vmem] * 6 + [pl.BlockSpec(memory_space=pl.ANY)],
        out_specs=[vmem] * 4,
        scratch_shapes=[
            blocks,
            blocks,
            blocks,
            blocks,
            blocks,
            blocks,
            pltpu.VMEM((tokens, heads * count * lanes), half),
            pltpu.VMEM((tokens, model), jnp.float32),
            pltpu.VMEM(out_weight.shape, half),
            dma,
            dma((heads, 3, count)),
            dma((heads, 3, count)),
            dma((heads, count)),
            dma((heads, count)),
        ],
        compiler_params=pltpu.CompilerParams(
            collective_id=2, has_side_effects=True, vmem_limit_bytes=60 * 1024 * 1024
        ),
        name="attention",
    )(
        queries,
        keys,
        values,
        cos_table,
        sin_table,
        lambdas,
        head_gain[None, :],
        residual,
        mixer_gain[None, :],
        channel_gain[None, :],
        routes,
        logits,
        out_weight,
    )


def expert_kernel(
    count,
    groups,
    rows_ref,
    place_ref,
    mix_ref,
    stream_ref,
    gain_ref,
    gate_hbm,
    up_hbm,
    down_hbm,
    out_ref,
    outgoing,
    arrived,
    own,
    pair_in,
    cross_in,
    final,
    returned,
    hidden,
    gate_w,
    up_w,
    down_w,
    w_sem,
    a_send,
    a_recv,
    b_send,
    b_recv,
    c_send,
    c_recv,
    d_send,
    d_recv,
    e_send,
    e_recv,
    f_send,
    f_recv,
):
    me = lax.axis_index("sp")
    dp = lax.axis_index("dp")
    chip, core = dp // 2, dp % 2
    other = {"sp": me, "dp": chip * 2 + (1 - core)}

    def chip_at(step):
        return {"sp": me, "dp": ((chip + step + groups) % groups) * 2 + core}

    def far(k):
        return count // 2 + (k // 2) * (2 * (k % 2) - 1)

    def sp_at(step):
        return {"sp": (me + step + count) % count, "dp": dp}

    def remote(src, dst, send, recv, device):
        return pltpu.make_async_remote_copy(
            src_ref=src, dst_ref=dst, send_sem=send, recv_sem=recv, device_id=device, device_id_type=MESH
        )

    def send_out(k):
        return remote(outgoing.at[k], arrived.at[k, 0, 0], a_send.at[k], a_recv.at[k], sp_at(far(k)))

    def cross_out(k, j):
        return remote(arrived.at[k, 0, 0], arrived.at[k, 0, j], b_send.at[k, j], b_recv.at[k, j], chip_at(j))

    def twin_out(k, j):
        return remote(arrived.at[k, 0, j], arrived.at[k, 1, j], c_send.at[k, j], c_recv.at[k, j], other)

    def pair_out(k):
        return remote(arrived.at[k, 1], pair_in.at[k], d_send.at[k], d_recv.at[k], other)

    def cross_back(k, j):
        return remote(own.at[k, j], cross_in.at[k, j], e_send.at[k, j], e_recv.at[k, j], chip_at(-j))

    def send_back(k):
        return remote(final.at[k], returned.at[k], f_send.at[k], f_recv.at[k], sp_at(-far(k)))

    weights = [
        pltpu.make_async_copy(hbm, vmem, w_sem.at[i])
        for i, (hbm, vmem) in enumerate(((gate_hbm, gate_w), (up_hbm, up_w), (down_hbm, down_w)))
    ]
    for copy in weights:
        copy.start()

    barrier = pltpu.get_barrier_semaphore()
    peers = [sp_at(k) for k in range(1, count)] + [chip_at(j) for j in range(1, groups)] + [other]
    for peer in peers:
        pl.semaphore_signal(barrier, inc=1, device_id=peer, device_id_type=MESH)

    capacity = outgoing.shape[1]
    model = rows_ref.shape[1]
    units = gate_w.shape[1]
    wide = math.gcd(model, 512)

    @pl.loop(0, model // wide)
    def _(n):
        cols = pl.ds(pl.multiple_of(n * wide, wide), wide)
        block = lax.dot_general(
            place_ref[...], rows_ref[:, cols], (((0,), (0,)), ((), ())), preferred_element_type=jnp.float32
        )
        block = block.astype(jnp.bfloat16).reshape(count, capacity, wide)
        arrived[0, 0, 0, :, cols] = block[0]
        outgoing[:, :, cols] = block

    pl.semaphore_wait(barrier, len(peers))

    @pl.loop(1, count)
    def _(k):
        send_out(k).start()

    width = 1
    rounds = count // width

    def per_k(group, action):
        for i in range(width):
            action(group * width + i)

    def forward(k):
        @pl.when(k > 0)
        def _():
            send_out(k).wait_recv()

        for j in range(1, groups):
            cross_out(k, j).start()
        twin_out(k, 0).start()

    def forward_twin(k):
        for j in range(1, groups):
            cross_out(k, j).wait_recv()
            twin_out(k, j).start()

    def complete(k):
        for j in range(groups):
            twin_out(k, j).wait_recv()

    def pair_sum(k):
        pair_out(k).wait_recv()
        for j in range(groups):
            own[k, j] = (own[k, j].astype(jnp.float32) + pair_in[k, j].astype(jnp.float32)).astype(jnp.bfloat16)
        for j in range(1, groups):
            cross_back(k, j).start()

    def total(k):
        value = own[k, 0].astype(jnp.float32)
        for j in range(1, groups):
            cross_back(k, j).wait_recv()
            value = value + cross_in[k, j].astype(jnp.float32)
        value = value.astype(jnp.bfloat16)

        @pl.when(k > 0)
        def _():
            final[k] = value
            send_back(k).start()

        @pl.when(k == 0)
        def _():
            returned[k] = value

    tile = math.gcd(units, 256)

    def compute(group):
        first = group * width
        held = width * 2 * groups * capacity
        slab = arrived.at[pl.ds(first, width)]

        @pl.loop(0, units // tile)
        def _(n):
            cols = pl.ds(pl.multiple_of(n * tile, tile), tile)
            value = slab[...].reshape(held, model)
            gate = jnp.dot(value, gate_w[:, cols], preferred_element_type=jnp.float32)
            up = jnp.dot(value, up_w[:, cols], preferred_element_type=jnp.float32)
            hidden[:, cols] = (gate / (1.0 + jnp.exp(-gate)) * up).astype(jnp.bfloat16)

        @pl.loop(0, model // wide)
        def _(n):
            cols = pl.ds(pl.multiple_of(n * wide, wide), wide)
            part = jnp.dot(hidden[...], down_w[:, cols], preferred_element_type=jnp.float32)
            part = part.astype(jnp.bfloat16).reshape(width, 2, groups, capacity, wide)
            for i in range(width):
                own[first + i, :, :, cols] = part[i, 0]
                arrived[first + i, 1, :, :, cols] = part[i, 1]

        per_k(group, lambda k: pair_out(k).start())

    @pl.loop(0, rounds + 3)
    def _(g):
        @pl.when(g < rounds)
        def _():
            per_k(g, forward)

        @pl.when((g >= 2) & (g < rounds + 2))
        def _():
            per_k(g - 2, pair_sum)

        @pl.when(g >= 3)
        def _():
            per_k(g - 3, total)

        @pl.when((g >= 1) & (g < rounds + 1))
        def _():
            @pl.when(g == 1)
            def _():
                for copy in weights:
                    copy.wait()

            per_k(g - 1, forward_twin)
            per_k(g - 1, complete)
            compute(g - 1)

    @pl.loop(1, count)
    def _(k):
        send_back(k).wait_recv()

    square = jnp.zeros((stream_ref.shape[0], 1), jnp.float32)
    share = mix_ref[...]
    high = share.astype(jnp.bfloat16)
    low = (share - high.astype(jnp.float32)).astype(jnp.bfloat16)
    pieces = []
    for n in range(model // wide):
        cols = slice(n * wide, (n + 1) * wide)
        back = returned[:, :, cols].reshape(count * capacity, wide)
        piece = jnp.dot(high, back, preferred_element_type=jnp.float32)
        piece = piece + jnp.dot(low, back, preferred_element_type=jnp.float32)
        square = square + jnp.sum(piece * piece, axis=-1, keepdims=True)
        pieces.append(piece)
    norm = lax.rsqrt(square / model + 1e-06)
    for n, piece in enumerate(pieces):
        cols = slice(n * wide, (n + 1) * wide)
        value = stream_ref[:, cols].astype(jnp.float32) + piece * norm * gain_ref[:, cols]
        out_ref[:, cols] = value.astype(jnp.bfloat16)

    @pl.loop(0, count)
    def _(k):
        @pl.when(k > 0)
        def _():
            send_out(k).wait_send()
            send_back(k).wait_send()

        for j in range(1, groups):
            cross_out(k, j).wait_send()
            cross_back(k, j).wait_send()
        for j in range(groups):
            twin_out(k, j).wait_send()
        pair_out(k).wait_send()


def expert_stage(normed, stream, place, mix, expert_gain, gate_weight, up_weight, down_weight):
    count, dp_count = lax.axis_size("sp"), lax.axis_size("dp")
    groups = dp_count // 2
    tokens, model = normed.shape
    units = gate_weight.shape[1]
    capacity = mix.shape[1] // count
    vmem, anywhere = pl.BlockSpec(memory_space=pltpu.VMEM), pl.BlockSpec(memory_space=pl.ANY)
    half = jnp.bfloat16
    dma = pltpu.SemaphoreType.DMA
    return pl.pallas_call(
        functools.partial(expert_kernel, count, groups),
        out_shape=jax.ShapeDtypeStruct((tokens, model), jnp.bfloat16),
        in_specs=[vmem] * 5 + [anywhere] * 3,
        out_specs=vmem,
        scratch_shapes=[
            pltpu.VMEM((count, capacity, model), half),
            pltpu.VMEM((count, 2, groups, capacity, model), half),
            pltpu.VMEM((count, groups, capacity, model), half),
            pltpu.VMEM((count, groups, capacity, model), half),
            pltpu.VMEM((count, groups, capacity, model), half),
            pltpu.VMEM((count, capacity, model), half),
            pltpu.VMEM((count, capacity, model), half),
            pltpu.VMEM((2 * groups * capacity, units), half),
            pltpu.VMEM((model, units), half),
            pltpu.VMEM((model, units), half),
            pltpu.VMEM((units, model), half),
            dma((3,)),
            dma((count,)),
            dma((count,)),
            dma((count, groups)),
            dma((count, groups)),
            dma((count, groups)),
            dma((count, groups)),
            dma((count,)),
            dma((count,)),
            dma((count, groups)),
            dma((count, groups)),
            dma((count,)),
            dma((count,)),
        ],
        compiler_params=pltpu.CompilerParams(
            collective_id=1, has_side_effects=True, vmem_limit_bytes=67043328
        ),
        name="experts",
    )(normed, place, mix, stream, expert_gain[None, :], gate_weight, up_weight, down_weight)


def local(
    queries,
    key_rows,
    value_rows,
    lambdas,
    head_gain,
    out_weight,
    residual,
    mixer_gain,
    channel_gain,
    expert_gain,
    routes,
    route_logits,
    gate_weight,
    up_weight,
    down_weight,
):
    stream, normed, place, mix = attention_stage(
        queries[0],
        key_rows[0],
        value_rows[0],
        lambdas,
        head_gain,
        out_weight,
        residual[0],
        mixer_gain,
        channel_gain,
        routes[0],
        route_logits[0],
    )
    updated = expert_stage(
        normed,
        stream,
        place,
        mix,
        expert_gain,
        gate_weight[0],
        up_weight[0],
        down_weight[0],
    )
    return updated[None]


def solution(mesh):
    placed = (
        P("dp", "sp", None),
        P("dp", "sp", None),
        P("dp", "sp", None),
        P("sp"),
        P(),
        P(),
        P("dp", "sp", None),
        P(),
        P(),
        P(),
        P("dp", "sp", None),
        P("dp", "sp", None),
        P("sp", None, "dp"),
        P("sp", None, "dp"),
        P("sp", "dp", None),
    )
    return jax.shard_map(
        local, mesh=mesh, in_specs=placed, out_specs=P("dp", "sp", None), check_vma=False
    )
```

profile of v0, /device:TPU:0, one launch (start us, length us, event | category | flops | bytes accessed | tf_op | source)
XLA Modules:
  0.0 170.7 jit_solution(5632912730630555444)
XLA Ops:
  0.0 1.4 copy.19
  1.4 1.4 copy.20
  2.8 0.3 fusion
  3.2 0.8 pad_maximum_fusion
  4.0 60.5 %attention.1 = (bf16[128,2048]{1,0:T(8,128)(2,1)}, bf16[128,2048]{1,0:T(8,128)(2,1)}, bf16[128,384]{1,0:T(8,128)(2,1)}, f32[128,384]{1,0:T(8,128)}) custom-call(bf16[128,2048]{1,0:T(8,128)(2,1)} %bitcast.18, bf16[128,2048]{1,0:T(8,128)(2,1)} %bitcast.19, bf16[128,2048]{1,0:T(8,128)(2,1)} %bitcast.20, f32[128,128]{1,0:T(8,128)} %get-tuple-element.16.cos_ref, ...), custom_call_target="tpu_custom_call" | custom-call | tf_op jit(solution)/shard_map/attention/pallas_call | solution.py:275
  64.5 104.3 %experts.1 = bf16[128,2048]{1,0:T(8,128)(2,1)} custom-call(bf16[128,2048]{1,0:T(8,128)(2,1)} %get-tuple-element.9.rows_ref, bf16[128,384]{1,0:T(8,128)(2,1)} %get-tuple-element.10.place_ref, f32[128,384]{1,0:T(8,128)} %get-tuple-element.11.mix_ref, bf16[128,2048]{1,0:T(8,128)(2,1)} %get-tuple-element.12.stream_ref, f32[1,2048]{1,0:T(1,128)} %bitcast.24, ...), custom_call_target="tpu_custom_call" | custom-call | tf_op jit(solution)/shard_map/experts/pallas_call | solution.py:574
  168.8 1.9 %copy.22 = bf16[1,128,2048]{2,1,0:T(8,128)(2,1)} copy(bf16[1,128,2048]{2,1,0:T(8,128)(2,1)} %bitcast.17) | data formatting | bytes 1048576
  (2 shorter events, 0.0 us)
where the time goes:
time: 171 us
  Pallas kernels  165 us (96%)
  local copies, waits for them, and re-layouts  4.71 us (3%)
    pallas_call x1, Pallas kernels, expert_stage(): pl.pallas_call(functools.partial(expert_kernel, count, groups), out_shape...  104 us
    pallas_call x1, Pallas kernels, attention_stage(): pl.pallas_call(functools.partial(attention_kernel, count, heads), out_sha...  60.5 us
    unnamed x3, local copies, waits for them, and re-layouts  4.71 us

commit v1 on v0

v1 whole, which is shorter than its diff:
```python
import functools
import math

import jax
import jax.numpy as jnp
import numpy as np
from jax import lax
from jax.experimental import pallas as pl
from jax.experimental.pallas import tpu as pltpu
from jax.sharding import PartitionSpec as P


MESH = pl.DeviceIdType.MESH
WIDTH = 2


def layer_kernel(
    count,
    groups,
    query_hbm,
    key_hbm,
    value_hbm,
    cos_hbm,
    sin_hbm,
    lambda_ref,
    head_gain_ref,
    residual_hbm,
    mixer_gain_ref,
    channel_gain_ref,
    expert_gain_ref,
    routes_ref,
    logits_ref,
    weight_hbm,
    gate_hbm,
    up_hbm,
    down_hbm,
    out_hbm,
    query_ref,
    key_ref,
    value_ref,
    cos_ref,
    sin_ref,
    residual_ref,
    query_out,
    key_out,
    query_in,
    key_in,
    value_in,
    head_out,
    token_rows,
    projected,
    square_ref,
    stream_ref,
    normed_ref,
    place_ref,
    high_ref,
    low_ref,
    pool,
    outgoing,
    arrived,
    own,
    cross_in,
    returned,
    hidden,
    gate_w,
    up_w,
    down_w,
    in_sem,
    weight_sem,
    expert_sem,
    out_sem,
    in_send,
    in_recv,
    head_send,
    head_recv,
    a_send,
    a_recv,
    b_send,
    b_recv,
    c_send,
    c_recv,
    d_send,
    d_recv,
    e_send,
    e_recv,
    f_send,
    f_recv,
):
    me = lax.axis_index("sp")
    dp = lax.axis_index("dp")
    chip, core = dp // 2, dp % 2
    tokens, model = query_ref.shape
    lanes = head_gain_ref.shape[1]
    heads = lambda_ref.shape[0]
    map_dim = lanes // 2
    scale = map_dim ** (-0.5)
    capacity = outgoing.shape[1]
    units = gate_w.shape[1]
    wide = math.gcd(model, 512)
    half = jnp.bfloat16

    def peer(k):
        total, bit = 0, 1
        while bit < count:
            a, b = (me // bit) % 2, (k // bit) % 2
            total = total + bit * (a + b - 2 * a * b)
            bit *= 2
        return total

    other = {"sp": me, "dp": chip * 2 + (1 - core)}

    def chip_at(step):
        return {"sp": me, "dp": ((chip + step + groups) % groups) * 2 + core}

    def sp_at(k):
        return {"sp": peer(k), "dp": dp}

    def columns(owner, h):
        return pl.ds(pl.multiple_of((owner * heads + h) * lanes, lanes), lanes)

    def tile_of(n, size):
        return pl.ds(pl.multiple_of(n * size, size), size)

    def remote(src, dst, send, recv, device):
        return pltpu.make_async_remote_copy(
            src_ref=src, dst_ref=dst, send_sem=send, recv_sem=recv, device_id=device, device_id_type=MESH
        )

    rows_here = pl.ds(pl.multiple_of(me * tokens, tokens), tokens)
    inputs = [
        pltpu.make_async_copy(src, dst, in_sem.at[i])
        for i, (src, dst) in enumerate(
            (
                (value_hbm, value_ref),
                (key_hbm, key_ref),
                (cos_hbm.at[rows_here], cos_ref),
                (sin_hbm.at[rows_here], sin_ref),
                (query_hbm, query_ref),
                (residual_hbm, residual_ref),
            )
        )
    ]
    for copy in inputs:
        copy.start()

    def weight_load(h, o):
        return pltpu.make_async_copy(
            weight_hbm.at[columns(o, h)],
            pool.at[pl.ds(pl.multiple_of((h * count + o) * lanes, lanes), lanes)],
            weight_sem.at[h, o],
        )

    expert_loads = [
        pltpu.make_async_copy(src, dst, expert_sem.at[i])
        for i, (src, dst) in enumerate(((gate_hbm, gate_w), (up_hbm, up_w), (down_hbm, down_w)))
    ]

    barrier = pltpu.get_barrier_semaphore()
    peers = [sp_at(k) for k in range(1, count)] + [chip_at(j) for j in range(1, groups)] + [other]
    for device in peers:
        pl.semaphore_signal(barrier, inc=1, device_id=device, device_id_type=MESH)

    def inward(h, k, i):
        sources = (value_ref.at[:, columns(peer(k), h)], query_out.at[h, k], key_out.at[h, k])
        targets = (value_in.at[h, k], query_in.at[h, k], key_in.at[h, k])
        return remote(sources[i], targets[i], in_send.at[h, i, k], in_recv.at[h, i, k], sp_at(k))

    def outward(h, k):
        return remote(
            head_out.at[h, k],
            token_rows.at[h, :, tile_of(me, lanes)],
            head_send.at[h, k],
            head_recv.at[h, k],
            sp_at(k),
        )

    first_half = lax.broadcasted_iota(jnp.int32, (tokens, lanes), 1) % map_dim < map_dim // 2

    def turned(ref, cols):
        x = ref[:, cols].astype(jnp.float32)
        ahead = pltpu.roll(x, lanes - map_dim // 2, 1)
        behind = pltpu.roll(x, map_dim // 2, 1)
        return x * cos_ref[...] + jnp.where(first_half, ahead, behind) * sin_ref[...]

    def turned_query(cols):
        return (turned(query_ref, cols) * scale).astype(half)

    def turned_key(cols):
        return turned(key_ref, cols).astype(half)

    inputs[0].wait()
    pl.semaphore_wait(barrier, len(peers))

    for h in range(heads):

        @pl.loop(1, count)
        def _(k):
            inward(h, k, 0).start()

        if h == 0:
            for copy in inputs[1:4]:
                copy.wait()

        @pl.loop(1, count)
        def _(k):
            key_out[h, k] = turned_key(columns(peer(k), h))

        @pl.loop(1, count)
        def _(k):
            inward(h, k, 2).start()

        if h == 0:
            inputs[4].wait()

        @pl.loop(1, count)
        def _(k):
            query_out[h, k] = turned_query(columns(peer(k), h))

        @pl.loop(1, count)
        def _(k):
            inward(h, count - k, 1).start()

    for h in range(heads):
        query_in[h, 0] = turned_query(columns(me, h))
        key_in[h, 0] = turned_key(columns(me, h))
        value_in[h, 0] = value_ref[:, columns(me, h)]

    for h in range(heads):

        @pl.loop(0, count)
        def _(o):
            weight_load(h, o).start()

    for copy in expert_loads:
        copy.start()

    top = routes_ref.shape[0]
    slots = count * capacity
    ranks = max(16, count)
    experts = lax.broadcasted_iota(jnp.int32, (ranks, tokens), 0)
    places = lax.broadcasted_iota(jnp.int32, (slots, tokens), 0)
    upper = lax.broadcasted_iota(jnp.int32, (tokens, tokens), 0)
    upper = (upper <= lax.broadcasted_iota(jnp.int32, (tokens, tokens), 1)).astype(half)
    logits = logits_ref[...]
    odds = jnp.exp(logits - jnp.max(logits, axis=0, keepdims=True))
    shares = odds / jnp.sum(odds, axis=0, keepdims=True)
    used = jnp.zeros((ranks, 1), jnp.float32)
    mix = jnp.zeros((slots, tokens), jnp.float32)
    place = jnp.zeros((slots, tokens), jnp.float32)
    for i in range(top):
        ranked = jnp.bitwise_xor(routes_ref[i : i + 1, :], me)
        named = (experts == ranked).astype(jnp.float32)
        running = jnp.dot(named.astype(half), upper, preferred_element_type=jnp.float32)
        slot = jnp.sum(named * (running + used), axis=0, keepdims=True).astype(jnp.int32) - 1
        used = used + jnp.sum(named, axis=1, keepdims=True)
        hit = places == ranked * capacity + slot
        mix = mix + jnp.where(hit, shares[i : i + 1, :], 0.0)
        place = place + jnp.where(hit, 1.0, 0.0)
    place_ref[...] = place.astype(half)
    mix = mix.T
    high = mix.astype(half)
    high_ref[...] = high
    low_ref[...] = (mix - high.astype(jnp.float32)).astype(half)

    rows = WIDTH * tokens
    length = count * tokens
    in_first = lax.broadcasted_iota(jnp.int32, (rows, lanes), 1) < map_dim

    def part_of(total):
        return jnp.exp(total - jnp.max(total, axis=-1, keepdims=True))

    for h in range(heads):

        @pl.loop(1, count)
        def _(k):
            inward(h, k, 0).wait_recv()
            inward(h, k, 2).wait_recv()

        @pl.loop(0, count // WIDTH)
        def _(step):
            b = count // WIDTH - 1 - step
            for i in range(WIDTH):
                k = b * WIDTH + i

                @pl.when(k > 0)
                def _():
                    inward(h, k, 1).wait_recv()

            query = query_in[h, pl.ds(b * WIDTH, WIDTH)].reshape(rows, lanes).astype(jnp.float32)
            both = jnp.concatenate(
                [jnp.where(in_first, query, 0.0), jnp.where(in_first, 0.0, query)], axis=0
            ).astype(half)
            keys = key_in[h].reshape(length, lanes)
            scores = lax.dot_general(
                both, keys, (((1,), (1,)), ((), ())), preferred_element_type=jnp.float32
            )
            one, two = part_of(scores[:rows]), part_of(scores[rows:])
            one_scale = 1.0 / jnp.sum(one, axis=-1, keepdims=True)
            two_scale = lambda_ref[h] / jnp.sum(two, axis=-1, keepdims=True)
            mixing = (one * one_scale - two * two_scale).astype(half)
            mixed = jnp.dot(
                mixing, value_in[h].reshape(length, lanes), preferred_element_type=jnp.float32
            )
            norm = lax.rsqrt(jnp.mean(mixed * mixed, axis=-1, keepdims=True) + 1e-05)
            result = (mixed * norm * head_gain_ref[...]).astype(half)
            head_out[h, pl.ds(b * WIDTH, WIDTH)] = result.reshape(WIDTH, tokens, lanes)
            for i in range(WIDTH):
                k = b * WIDTH + i

                @pl.when(k > 0)
                def _():
                    outward(h, k).start()

    for h in range(heads):
        token_rows[h, :, tile_of(me, lanes)] = head_out[h, 0]

    depth = count * lanes
    square_ref[...] = jnp.zeros_like(square_ref)

    def squares(value):
        value = value * value
        total = value[:, :128]
        for i in range(1, wide // 128):
            total = total + value[:, i * 128 : (i + 1) * 128]
        square_ref[...] += total

    def inverse_root():
        total = jnp.sum(square_ref[...], axis=-1, keepdims=True)
        return lax.rsqrt(total / model + 1e-06)

    for h in range(heads):

        @pl.loop(0, count)
        def _(o):
            weight_load(h, o).wait()

        @pl.loop(1, count)
        def _(k):
            outward(h, k).wait_recv()

        @pl.loop(0, model // wide)
        def _(n):
            cols = tile_of(n, wide)
            value = jnp.dot(
                token_rows[h], pool[h * depth : (h + 1) * depth, cols], preferred_element_type=jnp.float32
            )
            if h > 0:
                value = value + projected[:, cols]
            projected[:, cols] = value
            if h == heads - 1:
                squares(value)

    norm = inverse_root()
    square_ref[...] = jnp.zeros_like(square_ref)
    inputs[5].wait()

    @pl.loop(0, model // wide)
    def _(n):
        cols = tile_of(n, wide)
        stream = residual_ref[:, cols].astype(jnp.float32)
        stream = stream + projected[:, cols] * norm * mixer_gain_ref[:, cols]
        stream = stream.astype(half)
        stream_ref[:, cols] = stream
        squares(stream.astype(jnp.float32))

    norm2 = inverse_root()

    @pl.loop(0, model // wide)
    def _(n):
        cols = tile_of(n, wide)
        normed = stream_ref[:, cols].astype(jnp.float32) * norm2 * channel_gain_ref[:, cols]
        normed_ref[:, cols] = normed.astype(half)

    def send_out(k):
        return remote(outgoing.at[k], arrived.at[k, 0, 0], a_send.at[k], a_recv.at[k], sp_at(k))

    def cross_out(k, j):
        return remote(arrived.at[k, 0, 0], arrived.at[k, 0, j], b_send.at[k, j], b_recv.at[k, j], chip_at(j))

    def twin_out(k, j):
        return remote(arrived.at[k, 0, j], arrived.at[k, 1, j], c_send.at[k, j], c_recv.at[k, j], other)

    def pair_rows(k, j):
        return pl.ds(pl.multiple_of((k * groups + j) * capacity, capacity), capacity)

    def pair_out(k, j):
        return remote(arrived.at[k, 1, j], pool.at[pair_rows(k, j)], d_send.at[k, j], d_recv.at[k, j], other)

    def cross_back(k, j):
        return remote(own.at[k, j], cross_in.at[k, j - 1], e_send.at[k, j], e_recv.at[k, j], chip_at(-j))

    def send_back(k):
        return remote(own.at[k, 0], returned.at[k], f_send.at[k], f_recv.at[k], sp_at(k))

    near = count // 2

    def gather(first):
        @pl.loop(0, model // wide)
        def _(n):
            cols = tile_of(n, wide)
            chosen = place_ref[first * capacity : (first + near) * capacity, :]
            block = jnp.dot(chosen, normed_ref[:, cols], preferred_element_type=jnp.float32)
            block = block.astype(half).reshape(near, capacity, wide)
            outgoing[first : first + near, :, cols] = block
            if first == 0:
                arrived[0, 0, 0, :, cols] = block[0]

    gather(0)

    @pl.loop(1, near)
    def _(k):
        send_out(k).start()

    gather(near)

    @pl.loop(near, count)
    def _(k):
        send_out(k).start()

    def forward(k):
        @pl.when(k > 0)
        def _():
            send_out(k).wait_recv()

        for j in range(1, groups):
            cross_out(k, j).start()
        twin_out(k, 0).start()

    def forward_twin(k):
        for j in range(1, groups):
            cross_out(k, j).wait_recv()
            twin_out(k, j).start()

    def complete(k):
        for j in range(groups):
            twin_out(k, j).wait_recv()

    def pair_sum(k):
        for j in range(groups):
            pair_out(k, j).wait_recv()
            given = pool[pair_rows(k, j), :].astype(jnp.float32)
            own[k, j] = (own[k, j].astype(jnp.float32) + given).astype(half)
        for j in range(1, groups):
            cross_back(k, j).start()

    def total(k):
        value = own[k, 0].astype(jnp.float32)
        for j in range(1, groups):
            cross_back(k, j).wait_recv()
            value = value + cross_in[k, j - 1].astype(jnp.float32)
        value = value.astype(half)

        @pl.when(k > 0)
        def _():
            own[k, 0] = value
            send_back(k).start()

        @pl.when(k == 0)
        def _():
            returned[k] = value

    tile = math.gcd(units, 256)
    held = 2 * groups * capacity

    def compute(k):
        @pl.loop(0, units // tile)
        def _(n):
            cols = tile_of(n, tile)
            value = arrived[k].reshape(held, model)
            gate = jnp.dot(value, gate_w[:, cols], preferred_element_type=jnp.float32)
            up = jnp.dot(value, up_w[:, cols], preferred_element_type=jnp.float32)
            hidden[:, cols] = (gate / (1.0 + jnp.exp(-gate)) * up).astype(half)

        @pl.loop(0, model // wide)
        def _(n):
            cols = tile_of(n, wide)
            part = jnp.dot(hidden[...], down_w[:, cols], preferred_element_type=jnp.float32)
            part = part.astype(half).reshape(2, groups, capacity, wide)
            own[k, :, :, cols] = part[0]
            arrived[k, 1, :, :, cols] = part[1]

        for j in range(groups):
            pair_out(k, j).start()

    for copy in expert_loads:
        copy.wait()

    @pl.loop(0, count + 3)
    def _(g):
        @pl.when(g < count)
        def _():
            forward(g)

        @pl.when((g >= 2) & (g < count + 2))
        def _():
            pair_sum(g - 2)

        @pl.when(g >= 3)
        def _():
            total(g - 3)

        @pl.when((g >= 1) & (g < count + 1))
        def _():
            forward_twin(g - 1)
            complete(g - 1)
            compute(g - 1)

    square_ref[...] = jnp.zeros_like(square_ref)

    @pl.loop(1, count)
    def _(k):
        send_back(k).wait_recv()

    @pl.loop(0, model // wide)
    def _(n):
        cols = tile_of(n, wide)
        back = returned[:, :, cols].reshape(slots, wide)
        piece = jnp.dot(high_ref[...], back, preferred_element_type=jnp.float32)
        piece = piece + jnp.dot(low_ref[...], back, preferred_element_type=jnp.float32)
        projected[:, cols] = piece
        squares(piece)

    norm3 = inverse_root()

    def out_copy(n):
        cols = tile_of(n, wide)
        return pltpu.make_async_copy(normed_ref.at[:, cols], out_hbm.at[:, cols], out_sem.at[n])

    @pl.loop(0, model // wide)
    def _(n):
        cols = tile_of(n, wide)
        value = stream_ref[:, cols].astype(jnp.float32)
        value = value + projected[:, cols] * norm3 * expert_gain_ref[:, cols]
        normed_ref[:, cols] = value.astype(half)
        out_copy(n).start()

    for h in range(heads):

        @pl.loop(1, count)
        def _(k):
            for i in range(3):
                inward(h, k, i).wait_send()
            outward(h, k).wait_send()

    @pl.loop(0, count)
    def _(k):
        @pl.when(k > 0)
        def _():
            send_out(k).wait_send()
            send_back(k).wait_send()

        for j in range(1, groups):
            cross_out(k, j).wait_send()
            cross_back(k, j).wait_send()
        for j in range(groups):
            twin_out(k, j).wait_send()
            pair_out(k, j).wait_send()

    @pl.loop(0, model // wide)
    def _(n):
        out_copy(n).wait()


def local(
    queries,
    key_rows,
    value_rows,
    lambdas,
    head_gain,
    out_weight,
    residual,
    mixer_gain,
    channel_gain,
    expert_gain,
    routes,
    route_logits,
    gate_weight,
    up_weight,
    down_weight,
):
    count, groups = lax.axis_size("sp"), lax.axis_size("dp") // 2
    heads = lambdas.shape[0]
    lanes = head_gain.shape[0]
    map_dim = lanes // 2
    _, tokens, model = residual.shape
    units = gate_weight.shape[2]
    capacity = -(-max(2, 3 * tokens // count) // 16) * 16
    slots = count * capacity
    inverse = 1.0 / np.float32(10000.0) ** (np.arange(0, map_dim, 2, dtype=np.float32) / np.float32(map_dim))
    angles = np.arange(count * tokens, dtype=np.float32)[:, None] * inverse.astype(np.float32)[None, :]
    cosine = np.cos(angles.astype(np.float64)).astype(np.float32)
    sine = np.sin(angles.astype(np.float64)).astype(np.float32)
    cos_table = jnp.asarray(np.concatenate([cosine] * 4, axis=1))
    sin_table = jnp.asarray(np.concatenate([-sine, sine] * 2, axis=1))
    vmem = pl.BlockSpec(memory_space=pltpu.VMEM)
    smem = pl.BlockSpec(memory_space=pltpu.SMEM)
    anywhere = pl.BlockSpec(memory_space=pl.ANY)
    half = jnp.bfloat16
    dma = pltpu.SemaphoreType.DMA
    rows = pltpu.VMEM((tokens, model), half)
    blocks = pltpu.VMEM((heads, count, tokens, lanes), half)
    table = pltpu.VMEM((tokens, lanes), jnp.float32)
    pool_rows = max(out_weight.shape[0], slots * groups)
    wide = math.gcd(model, 512)
    updated = pl.pallas_call(
        functools.partial(layer_kernel, count, groups),
        out_shape=jax.ShapeDtypeStruct((tokens, model), half),
        in_specs=[anywhere] * 5 + [smem, vmem, anywhere] + [vmem] * 5 + [anywhere] * 4,
        out_specs=anywhere,
        scratch_shapes=[
            rows,
            rows,
            rows,
            table,
            table,
            rows,
            blocks,
            blocks,
            blocks,
            blocks,
            blocks,
            blocks,
            pltpu.VMEM((heads, tokens, count * lanes), half),
            pltpu.VMEM((tokens, model), jnp.float32),
            pltpu.VMEM((tokens, 128), jnp.float32),
            rows,
            rows,
            pltpu.VMEM((slots, tokens), half),
            pltpu.VMEM((tokens, slots), half),
            pltpu.VMEM((tokens, slots), half),
            pltpu.VMEM((pool_rows, model), half),
            pltpu.VMEM((count, capacity, model), half),
            pltpu.VMEM((count, 2, groups, capacity, model), half),
            pltpu.VMEM((count, groups, capacity, model), half),
            pltpu.VMEM((count, max(1, groups - 1), capacity, model), half),
            pltpu.VMEM((count, capacity, model), half),
            pltpu.VMEM((2 * groups * capacity, units), half),
            pltpu.VMEM((model, units), half),
            pltpu.VMEM((model, units), half),
            pltpu.VMEM((units, model), half),
            dma((6,)),
            dma((heads, count)),
            dma((3,)),
            dma((model // wide,)),
            dma((heads, 3, count)),
            dma((heads, 3, count)),
            dma((heads, count)),
            dma((heads, count)),
            dma((count,)),
            dma((count,)),
            dma((count, groups)),
            dma((count, groups)),
            dma((count, groups)),
            dma((count, groups)),
            dma((count, groups)),
            dma((count, groups)),
            dma((count, groups)),
            dma((count, groups)),
            dma((count,)),
            dma((count,)),
        ],
        compiler_params=pltpu.CompilerParams(
            collective_id=1, has_side_effects=True, vmem_limit_bytes=67043328
        ),
        name="layer",
    )(
        queries[0],
        key_rows[0],
        value_rows[0],
        cos_table,
        sin_table,
        lambdas,
        head_gain[None, :],
        residual[0],
        mixer_gain[None, :],
        channel_gain[None, :],
        expert_gain[None, :],
        routes[0].T,
        route_logits[0].T,
        out_weight,
        gate_weight[0],
        up_weight[0],
        down_weight[0],
    )
    return updated[None]


def solution(mesh):
    placed = (
        P("dp", "sp", None),
        P("dp", "sp", None),
        P("dp", "sp", None),
        P("sp"),
        P(),
        P(),
        P("dp", "sp", None),
        P(),
        P(),
        P(),
        P("dp", "sp", None),
        P("dp", "sp", None),
        P("sp", None, "dp"),
        P("sp", None, "dp"),
        P("sp", "dp", None),
    )
    return jax.shard_map(
        local, mesh=mesh, in_specs=placed, out_specs=P("dp", "sp", None), check_vma=False
    )
```

time: 171 us -> 153 us (0.89)
  the two profiles are of different devices: /device:TPU:0 before, /device:TPU:8 now
where the time goes in v1:
time: 153 us
  Pallas kernels  151 us (99%)
  local copies, waits for them, and re-layouts  1.88 us (1%)
    pallas_call x1, Pallas kernels, local(): pl.pallas_call(functools.partial(layer_kernel, count, groups), out_shape=...  151 us

profile of v1, /device:TPU:8, one launch (start us, length us, event | category | flops | bytes accessed | tf_op | source)
XLA Modules:
  0.0 152.5 jit_solution(6226673554192587086)
XLA Ops:
  0.0 150.6 %layer.1 = bf16[128,2048]{1,0:T(8,128)(2,1)} custom-call(bf16[128,2048]{1,0:T(8,128)(2,1)} %bitcast.22, bf16[128,2048]{1,0:T(8,128)(2,1)} %bitcast.23, bf16[128,2048]{1,0:T(8,128)(2,1)} %bitcast.24, f32[1024,128]{1,0:T(8,128)} %constant.4.clone.cos_hbm, f32[1024,128]{1,0:T(8,128)} %constant.5.clone.sin_hbm, f32[2]{0:T(128)} %lambda_ref.1, ...), custom_call_target="tpu_custom_call" | custom-call | tf_op jit(solution)/shard_map/layer/pallas_call | solution.py:605
  150.6 1.9 %copy.19 = bf16[1,128,2048]{2,1,0:T(8,128)(2,1)} copy(bf16[1,128,2048]{2,1,0:T(8,128)(2,1)} %bitcast.21) | data formatting | bytes 1048576

commit v2 on v1

--- a/solution.py
+++ b/solution.py
@@ -1,3 +1,4 @@
+import contextlib
 import functools
 import math
 
@@ -12,6 +13,40 @@
 
 MESH = pl.DeviceIdType.MESH
 WIDTH = 2
+TRACE = False
+
+
+def scope(name):
+    return jax.named_scope(name) if TRACE else contextlib.nullcontext()
+
+
+KINDS = "AYUDPT"
+INNER = (
+    "A1", "Y0", "U0", "D0", "A2", "Y1", "U1", "A4", "D1", "A3", "Y2", "U2", "Y4", "D2", "A5", "U4",
+    "D4", "Y3", "P4", "Y5", "A6", "U5", "A7", "D5", "T4", "U3", "P5", "P1", "D3", "Y6", "U6", "D6",
+    "T5", "P6", "P2", "Y7", "U7", "T6", "D7", "P7", "P3", "P0", "T1", "T2", "T7", "T3", "T0",
+)
+OUTER = (
+    "A1", "Y0", "U0", "D0", "A2", "Y1", "U1", "A4", "D1", "A3", "Y2", "U2", "Y4", "P1", "D2", "U4",
+    "A5", "D4", "Y3", "P4", "Y5", "U3", "A6", "D3", "U5", "T4", "D5", "A7", "P5", "Y6", "U6", "D6",
+    "T5", "P6", "P2", "Y7", "U7", "D7", "T6", "P7", "P3", "P0", "T1", "T7", "T2", "T3", "T0",
+)
+
+
+def plan(count, eight):
+    if count == 8:
+        return [(KINDS.index(step[0]), int(step[1:])) for step in eight]
+    steps = []
+    for n in range(count + 3):
+        if 0 < n < count:
+            steps.append((KINDS.index("A"), n))
+        if 2 <= n < count + 2:
+            steps.append((KINDS.index("P"), n - 2))
+        if n >= 3:
+            steps.append((KINDS.index("T"), n - 3))
+        if 1 <= n <= count:
+            steps += [(KINDS.index(kind), n - 1) for kind in "YUD"]
+    return steps
 
 
 def layer_kernel(
@@ -188,79 +223,82 @@
     def turned_key(cols):
         return turned(key_ref, cols).astype(half)
 
-    inputs[0].wait()
-    pl.semaphore_wait(barrier, len(peers))
-
-    for h in range(heads):
-
-        @pl.loop(1, count)
-        def _(k):
-            inward(h, k, 0).start()
-
-        if h == 0:
-            for copy in inputs[1:4]:
-                copy.wait()
-
-        @pl.loop(1, count)
-        def _(k):
-            key_out[h, k] = turned_key(columns(peer(k), h))
-
-        @pl.loop(1, count)
-        def _(k):
-            inward(h, k, 2).start()
-
-        if h == 0:
-            inputs[4].wait()
-
-        @pl.loop(1, count)
-        def _(k):
-            query_out[h, k] = turned_query(columns(peer(k), h))
-
-        @pl.loop(1, count)
-        def _(k):
-            inward(h, count - k, 1).start()
-
-    for h in range(heads):
-        query_in[h, 0] = turned_query(columns(me, h))
-        key_in[h, 0] = turned_key(columns(me, h))
-        value_in[h, 0] = value_ref[:, columns(me, h)]
-
-    for h in range(heads):
-
-        @pl.loop(0, count)
-        def _(o):
-            weight_load(h, o).start()
-
-    for copy in expert_loads:
-        copy.start()
-
-    top = routes_ref.shape[0]
-    slots = count * capacity
-    ranks = max(16, count)
-    experts = lax.broadcasted_iota(jnp.int32, (ranks, tokens), 0)
-    places = lax.broadcasted_iota(jnp.int32, (slots, tokens), 0)
-    upper = lax.broadcasted_iota(jnp.int32, (tokens, tokens), 0)
-    upper = (upper <= lax.broadcasted_iota(jnp.int32, (tokens, tokens), 1)).astype(half)
-    logits = logits_ref[...]
-    odds = jnp.exp(logits - jnp.max(logits, axis=0, keepdims=True))
-    shares = odds / jnp.sum(odds, axis=0, keepdims=True)
-    used = jnp.zeros((ranks, 1), jnp.float32)
-    mix = jnp.zeros((slots, tokens), jnp.float32)
-    place = jnp.zeros((slots, tokens), jnp.float32)
-    for i in range(top):
-        ranked = jnp.bitwise_xor(routes_ref[i : i + 1, :], me)
-        named = (experts == ranked).astype(jnp.float32)
-        running = jnp.dot(named.astype(half), upper, preferred_element_type=jnp.float32)
-        slot = jnp.sum(named * (running + used), axis=0, keepdims=True).astype(jnp.int32) - 1
-        used = used + jnp.sum(named, axis=1, keepdims=True)
-        hit = places == ranked * capacity + slot
-        mix = mix + jnp.where(hit, shares[i : i + 1, :], 0.0)
-        place = place + jnp.where(hit, 1.0, 0.0)
-    place_ref[...] = place.astype(half)
-    mix = mix.T
-    high = mix.astype(half)
-    high_ref[...] = high
-    low_ref[...] = (mix - high.astype(jnp.float32)).astype(half)
+    with scope("barrier"):
+        inputs[0].wait()
+        pl.semaphore_wait(barrier, len(peers))
+
+    with scope("prepare"):
+        for h in range(heads):
+
+            @pl.loop(1, count)
+            def _(k):
+                inward(h, k, 0).start()
+
+            if h == 0:
+                for copy in inputs[1:4]:
+                    copy.wait()
+
+            @pl.loop(1, count)
+            def _(k):
+                key_out[h, k] = turned_key(columns(peer(k), h))
+
+            @pl.loop(1, count)
+            def _(k):
+                inward(h, k, 2).start()
+
+            if h == 0:
+                inputs[4].wait()
+
+            @pl.loop(1, count)
+            def _(k):
+                query_out[h, k] = turned_query(columns(peer(k), h))
+
+            @pl.loop(1, count)
+            def _(k):
+                inward(h, count - k, 1).start()
+
+        for h in range(heads):
+            query_in[h, 0] = turned_query(columns(me, h))
+            key_in[h, 0] = turned_key(columns(me, h))
+            value_in[h, 0] = value_ref[:, columns(me, h)]
+
+        for h in range(heads):
+
+            @pl.loop(0, count)
+            def _(o):
+                weight_load(h, o).start()
+
+        for copy in expert_loads:
+            copy.start()
+
+    with scope("routing"):
+        top = routes_ref.shape[0]
+        slots = count * capacity
+        ranks = max(16, count)
+        experts = lax.broadcasted_iota(jnp.int32, (ranks, tokens), 0)
+        places = lax.broadcasted_iota(jnp.int32, (slots, tokens), 0)
+        upper = lax.broadcasted_iota(jnp.int32, (tokens, tokens), 0)
+        upper = (upper <= lax.broadcasted_iota(jnp.int32, (tokens, tokens), 1)).astype(half)
+        logits = logits_ref[...]
+        odds = jnp.exp(logits - jnp.max(logits, axis=0, keepdims=True))
+        shares = odds / jnp.sum(odds, axis=0, keepdims=True)
+        used = jnp.zeros((ranks, 1), jnp.float32)
+        mix = jnp.zeros((slots, tokens), jnp.float32)
+        place = jnp.zeros((slots, tokens), jnp.float32)
+        for i in range(top):
+            ranked = jnp.bitwise_xor(routes_ref[i : i + 1, :], me)
+            named = (experts == ranked).astype(jnp.float32)
+            running = jnp.dot(named.astype(half), upper, preferred_element_type=jnp.float32)
+            slot = jnp.sum(named * (running + used), axis=0, keepdims=True).astype(jnp.int32) - 1
+            used = used + jnp.sum(named, axis=1, keepdims=True)
+            hit = places == ranked * capacity + slot
+            mix = mix + jnp.where(hit, shares[i : i + 1, :], 0.0)
+            place = place + jnp.where(hit, 1.0, 0.0)
+        place_ref[...] = place.astype(half)
+        mix = mix.T
+        high = mix.astype(half)
+        high_ref[...] = high
+        low_ref[...] = (mix - high.astype(jnp.float32)).astype(half)
 
     rows = WIDTH * tokens
     length = count * tokens
@@ -271,39 +309,42 @@
 
     for h in range(heads):
 
-        @pl.loop(1, count)
-        def _(k):
-            inward(h, k, 0).wait_recv()
-            inward(h, k, 2).wait_recv()
+        with scope("wait_kv"):
+            @pl.loop(1, count)
+            def _(k):
+                inward(h, k, 0).wait_recv()
+                inward(h, k, 2).wait_recv()
 
         @pl.loop(0, count // WIDTH)
         def _(step):
             b = count // WIDTH - 1 - step
-            for i in range(WIDTH):
-                k = b * WIDTH + i
-
-                @pl.when(k > 0)
-                def _():
-                    inward(h, k, 1).wait_recv()
-
-            query = query_in[h, pl.ds(b * WIDTH, WIDTH)].reshape(rows, lanes).astype(jnp.float32)
-            both = jnp.concatenate(
-                [jnp.where(in_first, query, 0.0), jnp.where(in_first, 0.0, query)], axis=0
-            ).astype(half)
-            keys = key_in[h].reshape(length, lanes)
-            scores = lax.dot_general(
-                both, keys, (((1,), (1,)), ((), ())), preferred_element_type=jnp.float32
-            )
-            one, two = part_of(scores[:rows]), part_of(scores[rows:])
-            one_scale = 1.0 / jnp.sum(one, axis=-1, keepdims=True)
-            two_scale = lambda_ref[h] / jnp.sum(two, axis=-1, keepdims=True)
-            mixing = (one * one_scale - two * two_scale).astype(half)
-            mixed = jnp.dot(
-                mixing, value_in[h].reshape(length, lanes), preferred_element_type=jnp.float32
-            )
-            norm = lax.rsqrt(jnp.mean(mixed * mixed, axis=-1, keepdims=True) + 1e-05)
-            result = (mixed * norm * head_gain_ref[...]).astype(half)
-            head_out[h, pl.ds(b * WIDTH, WIDTH)] = result.reshape(WIDTH, tokens, lanes)
+            with scope("wait_q"):
+                for i in range(WIDTH):
+                    k = b * WIDTH + i
+
+                    @pl.when(k > 0)
+                    def _():
+                        inward(h, k, 1).wait_recv()
+
+            with scope("attend"):
+                query = query_in[h, pl.ds(b * WIDTH, WIDTH)].reshape(rows, lanes).astype(jnp.float32)
+                both = jnp.concatenate(
+                    [jnp.where(in_first, query, 0.0), jnp.where(in_first, 0.0, query)], axis=0
+                ).astype(half)
+                keys = key_in[h].reshape(length, lanes)
+                scores = lax.dot_general(
+                    both, keys, (((1,), (1,)), ((), ())), preferred_element_type=jnp.float32
+                )
+                one, two = part_of(scores[:rows]), part_of(scores[rows:])
+                one_scale = 1.0 / jnp.sum(one, axis=-1, keepdims=True)
+                two_scale = lambda_ref[h] / jnp.sum(two, axis=-1, keepdims=True)
+                mixing = (one * one_scale - two * two_scale).astype(half)
+                mixed = jnp.dot(
+                    mixing, value_in[h].reshape(length, lanes), preferred_element_type=jnp.float32
+                )
+                norm = lax.rsqrt(jnp.mean(mixed * mixed, axis=-1, keepdims=True) + 1e-05)
+                result = (mixed * norm * head_gain_ref[...]).astype(half)
+                head_out[h, pl.ds(b * WIDTH, WIDTH)] = result.reshape(WIDTH, tokens, lanes)
             for i in range(WIDTH):
                 k = b * WIDTH + i
 
@@ -334,42 +375,45 @@
         def _(o):
             weight_load(h, o).wait()
 
-        @pl.loop(1, count)
-        def _(k):
-            outward(h, k).wait_recv()
+        with scope("wait_heads"):
+            @pl.loop(1, count)
+            def _(k):
+                outward(h, k).wait_recv()
+
+        with scope("project"):
+            @pl.loop(0, model // wide)
+            def _(n):
+                cols = tile_of(n, wide)
+                value = jnp.dot(
+                    token_rows[h], pool[h * depth : (h + 1) * depth, cols], preferred_element_type=jnp.float32
+                )
+                if h > 0:
+                    value = value + projected[:, cols]
+                projected[:, cols] = value
+                if h == heads - 1:
+                    squares(value)
+
+    with scope("norms"):
+        norm = inverse_root()
+        square_ref[...] = jnp.zeros_like(square_ref)
+        inputs[5].wait()
 
         @pl.loop(0, model // wide)
         def _(n):
             cols = tile_of(n, wide)
-            value = jnp.dot(
-                token_rows[h], pool[h * depth : (h + 1) * depth, cols], preferred_element_type=jnp.float32
-            )
-            if h > 0:
-                value = value + projected[:, cols]
-            projected[:, cols] = value
-            if h == heads - 1:
-                squares(value)
-
-    norm = inverse_root()
-    square_ref[...] = jnp.zeros_like(square_ref)
-    inputs[5].wait()
-
-    @pl.loop(0, model // wide)
-    def _(n):
-        cols = tile_of(n, wide)
-        stream = residual_ref[:, cols].astype(jnp.float32)
-        stream = stream + projected[:, cols] * norm * mixer_gain_ref[:, cols]
-        stream = stream.astype(half)
-        stream_ref[:, cols] = stream
-        squares(stream.astype(jnp.float32))
-
-    norm2 = inverse_root()
-
-    @pl.loop(0, model // wide)
-    def _(n):
-        cols = tile_of(n, wide)
-        normed = stream_ref[:, cols].astype(jnp.float32) * norm2 * channel_gain_ref[:, cols]
-        normed_ref[:, cols] = normed.astype(half)
+            stream = residual_ref[:, cols].astype(jnp.float32)
+            stream = stream + projected[:, cols] * norm * mixer_gain_ref[:, cols]
+            stream = stream.astype(half)
+            stream_ref[:, cols] = stream
+            squares(stream.astype(jnp.float32))
+
+        norm2 = inverse_root()
+
+        @pl.loop(0, model // wide)
+        def _(n):
+            cols = tile_of(n, wide)
+            normed = stream_ref[:, cols].astype(jnp.float32) * norm2 * channel_gain_ref[:, cols]
+            normed_ref[:, cols] = normed.astype(half)
 
     def send_out(k):
         return remote(outgoing.at[k], arrived.at[k, 0, 0], a_send.at[k], a_recv.at[k], sp_at(k))
@@ -405,39 +449,45 @@
             if first == 0:
                 arrived[0, 0, 0, :, cols] = block[0]
 
-    gather(0)
-
-    @pl.loop(1, near)
-    def _(k):
-        send_out(k).start()
-
-    gather(near)
-
-    @pl.loop(near, count)
-    def _(k):
-        send_out(k).start()
-
     def forward(k):
         @pl.when(k > 0)
         def _():
-            send_out(k).wait_recv()
+            with scope("A_wait"):
+                send_out(k).wait_recv()
 
         for j in range(1, groups):
             cross_out(k, j).start()
         twin_out(k, 0).start()
 
+    with scope("gather"):
+        gather(0)
+
+        @pl.loop(1, near)
+        def _(k):
+            send_out(k).start()
+
+        forward(0)
+        gather(near)
+
+        @pl.loop(near, count)
+        def _(k):
+            send_out(k).start()
+
     def forward_twin(k):
         for j in range(1, groups):
-            cross_out(k, j).wait_recv()
+            with scope("Y_wait"):
+                cross_out(k, j).wait_recv()
             twin_out(k, j).start()
 
     def complete(k):
         for j in range(groups):
-            twin_out(k, j).wait_recv()
+            with scope("twin_wait"):
+                twin_out(k, j).wait_recv()
 
     def pair_sum(k):
         for j in range(groups):
-            pair_out(k, j).wait_recv()
+            with scope("pair_wait"):
+                pair_out(k, j).wait_recv()
             given = pool[pair_rows(k, j), :].astype(jnp.float32)
             own[k, j] = (own[k, j].astype(jnp.float32) + given).astype(half)
         for j in range(1, groups):
@@ -446,7 +496,8 @@
     def total(k):
         value = own[k, 0].astype(jnp.float32)
         for j in range(1, groups):
-            cross_back(k, j).wait_recv()
+            with scope("B_wait"):
+                cross_back(k, j).wait_recv()
             value = value + cross_in[k, j - 1].astype(jnp.float32)
         value = value.astype(half)
 
@@ -462,103 +513,107 @@
     tile = math.gcd(units, 256)
     held = 2 * groups * capacity
 
-    def compute(k):
-        @pl.loop(0, units // tile)
-        def _(n):
-            cols = tile_of(n, tile)
-            value = arrived[k].reshape(held, model)
-            gate = jnp.dot(value, gate_w[:, cols], preferred_element_type=jnp.float32)
-            up = jnp.dot(value, up_w[:, cols], preferred_element_type=jnp.float32)
-            hidden[:, cols] = (gate / (1.0 + jnp.exp(-gate)) * up).astype(half)
-
+    def expand(k):
+        complete(k)
+
+        with scope("ffn_up"):
+            @pl.loop(0, units // tile)
+            def _(n):
+                cols = tile_of(n, tile)
+                value = arrived[k].reshape(held, model)
+                gate = jnp.dot(value, gate_w[:, cols], preferred_element_type=jnp.float32)
+                up = jnp.dot(value, up_w[:, cols], preferred_element_type=jnp.float32)
+                hidden[:, cols] = (gate / (1.0 + jnp.exp(-gate)) * up).astype(half)
+
+    def contract(k):
+        with scope("ffn_down"):
+            @pl.loop(0, model // wide)
+            def _(n):
+                cols = tile_of(n, wide)
+                part = jnp.dot(hidden[...], down_w[:, cols], preferred_element_type=jnp.float32)
+                part = part.astype(half).reshape(2, groups, capacity, wide)
+                own[k, :, :, cols] = part[0]
+                arrived[k, 1, :, :, cols] = part[1]
+
+        for j in range(groups):
+            pair_out(k, j).start()
+
+    for copy in expert_loads:
+        copy.wait()
+
+    kinds = (forward, forward_twin, expand, contract, pair_sum, total)
+    inner, outer = ([kind * count + k for kind, k in plan(count, eight)] for eight in (INNER, OUTER))
+    ends = (me < count // 4) | (me >= count - count // 4)
+
+    @pl.loop(0, len(inner))
+    def _(i):
+        code = 0
+        for n in range(len(inner)):
+            value = inner[n] if inner[n] == outer[n] else jnp.where(ends, outer[n], inner[n])
+            code = jnp.where(i == n, value, code)
+        for kind, action in enumerate(kinds):
+
+            @pl.when(code // count == kind)
+            def _():
+                action(code % count)
+
+    square_ref[...] = jnp.zeros_like(square_ref)
+
+    with scope("wait_back"):
+        @pl.loop(1, count)
+        def _(k):
+            send_back(k).wait_recv()
+
+    with scope("combine"):
         @pl.loop(0, model // wide)
         def _(n):
             cols = tile_of(n, wide)
-            part = jnp.dot(hidden[...], down_w[:, cols], preferred_element_type=jnp.float32)
-            part = part.astype(half).reshape(2, groups, capacity, wide)
-            own[k, :, :, cols] = part[0]
-            arrived[k, 1, :, :, cols] = part[1]
-
-        for j in range(groups):
-            pair_out(k, j).start()
-
-    for copy in expert_loads:
-        copy.wait()
-
-    @pl.loop(0, count + 3)
-    def _(g):
-        @pl.when(g < count)
-        def _():
-            forward(g)
-
-        @pl.when((g >= 2) & (g < count + 2))
-        def _():
-            pair_sum(g - 2)
-
-        @pl.when(g >= 3)
-        def _():
-            total(g - 3)
-
-        @pl.when((g >= 1) & (g < count + 1))
-        def _():
-            forward_twin(g - 1)
-            complete(g - 1)
-            compute(g - 1)
-
-    square_ref[...] = jnp.zeros_like(square_ref)
-
-    @pl.loop(1, count)
-    def _(k):
-        send_back(k).wait_recv()
-
-    @pl.loop(0, model // wide)
-    def _(n):
-        cols = tile_of(n, wide)
-        back = returned[:, :, cols].reshape(slots, wide)
-        piece = jnp.dot(high_ref[...], back, preferred_element_type=jnp.float32)
-        piece = piece + jnp.dot(low_ref[...], back, preferred_element_type=jnp.float32)
-        projected[:, cols] = piece
-        squares(piece)
-
-    norm3 = inverse_root()
-
-    def out_copy(n):
-        cols = tile_of(n, wide)
-        return pltpu.make_async_copy(normed_ref.at[:, cols], out_hbm.at[:, cols], out_sem.at[n])
-
-    @pl.loop(0, model // wide)
-    def _(n):
-        cols = tile_of(n, wide)
-        value = stream_ref[:, cols].astype(jnp.float32)
-        value = value + projected[:, cols] * norm3 * expert_gain_ref[:, cols]
-        normed_ref[:, cols] = value.astype(half)
-        out_copy(n).start()
-
-    for h in range(heads):
-
-        @pl.loop(1, count)
+            back = returned[:, :, cols].reshape(slots, wide)
+            piece = jnp.dot(high_ref[...], back, preferred_element_type=jnp.float32)
+            piece = piece + jnp.dot(low_ref[...], back, preferred_element_type=jnp.float32)
+            projected[:, cols] = piece
+            squares(piece)
+
+        norm3 = inverse_root()
+
+        def out_copy(n):
+            cols = tile_of(n, wide)
+            return pltpu.make_async_copy(normed_ref.at[:, cols], out_hbm.at[:, cols], out_sem.at[n])
+
+        @pl.loop(0, model // wide)
+        def _(n):
+            cols = tile_of(n, wide)
+            value = stream_ref[:, cols].astype(jnp.float32)
+            value = value + projected[:, cols] * norm3 * expert_gain_ref[:, cols]
+            normed_ref[:, cols] = value.astype(half)
+            out_copy(n).start()
+
+    with scope("drain"):
+        for h in range(heads):
+
+            @pl.loop(1, count)
+            def _(k):
+                for i in range(3):
+                    inward(h, k, i).wait_send()
+                outward(h, k).wait_send()
+
+        @pl.loop(0, count)
         def _(k):
-            for i in range(3):
-                inward(h, k, i).wait_send()
-            outward(h, k).wait_send()
-
-    @pl.loop(0, count)
-    def _(k):
-        @pl.when(k > 0)
-        def _():
-            send_out(k).wait_send()
-            send_back(k).wait_send()
-
-        for j in range(1, groups):
-            cross_out(k, j).wait_send()
-            cross_back(k, j).wait_send()
-        for j in range(groups):
-            twin_out(k, j).wait_send()
-            pair_out(k, j).wait_send()
-
-    @pl.loop(0, model // wide)
-    def _(n):
-        out_copy(n).wait()
+            @pl.when(k > 0)
+            def _():
+                send_out(k).wait_send()
+                send_back(k).wait_send()
+
+            for j in range(1, groups):
+                cross_out(k, j).wait_send()
+                cross_back(k, j).wait_send()
+            for j in range(groups):
+                twin_out(k, j).wait_send()
+                pair_out(k, j).wait_send()
+
+        @pl.loop(0, model // wide)
+        def _(n):
+            out_copy(n).wait()
 
 
 def local(

time: 153 us -> 143 us (0.935)
  the two profiles are of different devices: /device:TPU:8 before, /device:TPU:0 now
where the time goes in v2:
time: 143 us
  Pallas kernels  141 us (99%)
  local copies, waits for them, and re-layouts  1.88 us (1%)
    pallas_call x1, Pallas kernels, local(): pl.pallas_call(functools.partial(layer_kernel, count, groups), out_shape=...  141 us

profile of v2, /device:TPU:0, one launch (start us, length us, event | category | flops | bytes accessed | tf_op | source)
XLA Modules:
  0.0 142.9 jit_solution(11441309762411192701)
XLA Ops:
  0.0 141.0 %layer.1 = bf16[128,2048]{1,0:T(8,128)(2,1)} custom-call(bf16[128,2048]{1,0:T(8,128)(2,1)} %bitcast.22, bf16[128,2048]{1,0:T(8,128)(2,1)} %bitcast.23, bf16[128,2048]{1,0:T(8,128)(2,1)} %bitcast.24, f32[1024,128]{1,0:T(8,128)} %constant.4.clone.cos_hbm, f32[1024,128]{1,0:T(8,128)} %constant.5.clone.sin_hbm, f32[2]{0:T(128)} %lambda_ref.1, ...), custom_call_target="tpu_custom_call" | custom-call | tf_op jit(solution)/shard_map/layer/pallas_call | solution.py:660
  141.0 1.9 %copy.19 = bf16[1,128,2048]{2,1,0:T(8,128)(2,1)} copy(bf16[1,128,2048]{2,1,0:T(8,128)(2,1)} %bitcast.21) | data formatting | bytes 1048576

commit v3 on v2

--- a/solution.py
+++ b/solution.py
@@ -105,7 +105,8 @@
     expert_sem,
     out_sem,
     in_send,
-    in_recv,
+    kv_recv,
+    query_recv,
     head_send,
     head_recv,
     a_send,
@@ -182,7 +183,7 @@
         return pltpu.make_async_copy(
             weight_hbm.at[columns(o, h)],
             pool.at[pl.ds(pl.multiple_of((h * count + o) * lanes, lanes), lanes)],
-            weight_sem.at[h, o],
+            weight_sem.at[h],
         )
 
     expert_loads = [
@@ -195,16 +196,20 @@
     for device in peers:
         pl.semaphore_signal(barrier, inc=1, device_id=device, device_id_type=MESH)
 
+    def wait_bytes(ref, sem):
+        pltpu.make_async_copy(ref, ref, sem).wait()
+
     def inward(h, k, i):
         sources = (value_ref.at[:, columns(peer(k), h)], query_out.at[h, k], key_out.at[h, k])
         targets = (value_in.at[h, k], query_in.at[h, k], key_in.at[h, k])
-        return remote(sources[i], targets[i], in_send.at[h, i, k], in_recv.at[h, i, k], sp_at(k))
+        landed = (kv_recv.at[h, 0], query_recv.at[h, k // WIDTH], kv_recv.at[h, 1])
+        return remote(sources[i], targets[i], in_send.at[h, i], landed[i], sp_at(k))
 
     def outward(h, k):
         return remote(
             head_out.at[h, k],
             token_rows.at[h, :, tile_of(me, lanes)],
-            head_send.at[h, k],
+            head_send.at[h],
             head_recv.at[h, k],
             sp_at(k),
         )
@@ -310,21 +315,20 @@
     for h in range(heads):
 
         with scope("wait_kv"):
-            @pl.loop(1, count)
-            def _(k):
-                inward(h, k, 0).wait_recv()
-                inward(h, k, 2).wait_recv()
+            wait_bytes(value_in.at[h, 1:count], kv_recv.at[h, 0])
+            wait_bytes(key_in.at[h, 1:count], kv_recv.at[h, 1])
 
         @pl.loop(0, count // WIDTH)
         def _(step):
             b = count // WIDTH - 1 - step
             with scope("wait_q"):
-                for i in range(WIDTH):
-                    k = b * WIDTH + i
-
-                    @pl.when(k > 0)
-                    def _():
-                        inward(h, k, 1).wait_recv()
+                @pl.when(b > 0)
+                def _():
+                    wait_bytes(query_in.at[h, pl.ds(b * WIDTH, WIDTH)], query_recv.at[h, b])
+
+                @pl.when(b == 0)
+                def _():
+                    wait_bytes(query_in.at[h, 1:WIDTH], query_recv.at[h, b])
 
             with scope("attend"):
                 query = query_in[h, pl.ds(b * WIDTH, WIDTH)].reshape(rows, lanes).astype(jnp.float32)
@@ -371,9 +375,7 @@
 
     for h in range(heads):
 
-        @pl.loop(0, count)
-        def _(o):
-            weight_load(h, o).wait()
+        wait_bytes(pool.at[h * depth : (h + 1) * depth], weight_sem.at[h])
 
         with scope("wait_heads"):
             @pl.loop(1, count)
@@ -416,25 +418,25 @@
             normed_ref[:, cols] = normed.astype(half)
 
     def send_out(k):
-        return remote(outgoing.at[k], arrived.at[k, 0, 0], a_send.at[k], a_recv.at[k], sp_at(k))
+        return remote(outgoing.at[k], arrived.at[k, 0, 0], a_send.at[0], a_recv.at[k], sp_at(k))
 
     def cross_out(k, j):
-        return remote(arrived.at[k, 0, 0], arrived.at[k, 0, j], b_send.at[k, j], b_recv.at[k, j], chip_at(j))
+        return remote(arrived.at[k, 0, 0], arrived.at[k, 0, j], b_send.at[0], b_recv.at[k, j - 1], chip_at(j))
 
     def twin_out(k, j):
-        return remote(arrived.at[k, 0, j], arrived.at[k, 1, j], c_send.at[k, j], c_recv.at[k, j], other)
+        return remote(arrived.at[k, 0, j], arrived.at[k, 1, j], c_send.at[0], c_recv.at[k], other)
 
     def pair_rows(k, j):
         return pl.ds(pl.multiple_of((k * groups + j) * capacity, capacity), capacity)
 
     def pair_out(k, j):
-        return remote(arrived.at[k, 1, j], pool.at[pair_rows(k, j)], d_send.at[k, j], d_recv.at[k, j], other)
+        return remote(arrived.at[k, 1, j], pool.at[pair_rows(k, j)], d_send.at[0], d_recv.at[k], other)
 
     def cross_back(k, j):
-        return remote(own.at[k, j], cross_in.at[k, j - 1], e_send.at[k, j], e_recv.at[k, j], chip_at(-j))
+        return remote(own.at[k, j], cross_in.at[k, j - 1], e_send.at[0], e_recv.at[k, j - 1], chip_at(-j))
 
     def send_back(k):
-        return remote(own.at[k, 0], returned.at[k], f_send.at[k], f_recv.at[k], sp_at(k))
+        return remote(own.at[k, 0], returned.at[k], f_send.at[0], f_recv.at[0], sp_at(k))
 
     near = count // 2
 
@@ -480,14 +482,14 @@
             twin_out(k, j).start()
 
     def complete(k):
+        with scope("twin_wait"):
+            wait_bytes(arrived.at[k, 1], c_recv.at[k])
+
+    def pair_sum(k):
+        held_rows = pl.ds(pl.multiple_of(k * groups * capacity, capacity), groups * capacity)
+        with scope("pair_wait"):
+            wait_bytes(pool.at[held_rows], d_recv.at[k])
         for j in range(groups):
-            with scope("twin_wait"):
-                twin_out(k, j).wait_recv()
-
-    def pair_sum(k):
-        for j in range(groups):
-            with scope("pair_wait"):
-                pair_out(k, j).wait_recv()
             given = pool[pair_rows(k, j), :].astype(jnp.float32)
             own[k, j] = (own[k, j].astype(jnp.float32) + given).astype(half)
         for j in range(1, groups):
@@ -560,9 +562,7 @@
     square_ref[...] = jnp.zeros_like(square_ref)
 
     with scope("wait_back"):
-        @pl.loop(1, count)
-        def _(k):
-            send_back(k).wait_recv()
+        wait_bytes(returned.at[1:count], f_recv.at[0])
 
     with scope("combine"):
         @pl.loop(0, model // wide)
@@ -578,7 +578,7 @@
 
         def out_copy(n):
             cols = tile_of(n, wide)
-            return pltpu.make_async_copy(normed_ref.at[:, cols], out_hbm.at[:, cols], out_sem.at[n])
+            return pltpu.make_async_copy(normed_ref.at[:, cols], out_hbm.at[:, cols], out_sem.at[0])
 
         @pl.loop(0, model // wide)
         def _(n):
@@ -590,30 +590,17 @@
 
     with scope("drain"):
         for h in range(heads):
-
-            @pl.loop(1, count)
-            def _(k):
-                for i in range(3):
-                    inward(h, k, i).wait_send()
-                outward(h, k).wait_send()
-
-        @pl.loop(0, count)
-        def _(k):
-            @pl.when(k > 0)
-            def _():
-                send_out(k).wait_send()
-                send_back(k).wait_send()
-
-            for j in range(1, groups):
-                cross_out(k, j).wait_send()
-                cross_back(k, j).wait_send()
-            for j in range(groups):
-                twin_out(k, j).wait_send()
-                pair_out(k, j).wait_send()
-
-        @pl.loop(0, model // wide)
-        def _(n):
-            out_copy(n).wait()
+            for i in range(3):
+                wait_bytes(value_in.at[h, 1:count], in_send.at[h, i])
+            wait_bytes(head_out.at[h, 1:count], head_send.at[h])
+        wait_bytes(outgoing.at[1:count], a_send.at[0])
+        if groups > 1:
+            wait_bytes(cross_in, b_send.at[0])
+            wait_bytes(cross_in, e_send.at[0])
+        wait_bytes(own, c_send.at[0])
+        wait_bytes(own, d_send.at[0])
+        wait_bytes(returned.at[1:count], f_send.at[0])
+        wait_bytes(normed_ref, out_sem.at[0])
 
 
 def local(
@@ -694,25 +681,26 @@
             pltpu.VMEM((model, units), half),
             pltpu.VMEM((units, model), half),
             dma((6,)),
+            dma((heads,)),
+            dma((3,)),
+            dma((1,)),
+            dma((heads, 3)),
+            dma((heads, 2)),
+            dma((heads, count // WIDTH)),
+            dma((heads,)),
             dma((heads, count)),
-            dma((3,)),
-            dma((model // wide,)),
-            dma((heads, 3, count)),
-            dma((heads, 3, count)),
-            dma((heads, count)),
-            dma((heads, count)),
+            dma((1,)),
             dma((count,)),
+            dma((1,)),
+            dma((count, max(1, groups - 1))),
+            dma((1,)),
             dma((count,)),
-            dma((count, groups)),
-            dma((count, groups)),
-            dma((count, groups)),
-            dma((count, groups)),
-            dma((count, groups)),
-            dma((count, groups)),
-            dma((count, groups)),
-            dma((count, groups)),
+            dma((1,)),
             dma((count,)),
-            dma((count,)),
+            dma((1,)),
+            dma((count, max(1, groups - 1))),
+            dma((1,)),
+            dma((1,)),
         ],
         compiler_params=pltpu.CompilerParams(
             collective_id=1, has_side_effects=True, vmem_limit_bytes=67043328

time: 143 us -> 141 us (0.986)
  Pallas kernels: 141 us -> 139 us
    pallas_call x1, Pallas kernels: 141 us -> 139 us  [local(): pl.pallas_call(functools.partial(layer_kernel, count, groups), out_shape=...]
where the time goes in v3:
time: 141 us
  Pallas kernels  139 us (99%)
  local copies, waits for them, and re-layouts  1.88 us (1%)
    pallas_call x1, Pallas kernels, local(): pl.pallas_call(functools.partial(layer_kernel, count, groups), out_shape=...  139 us

profile of v3, /device:TPU:0, one launch (start us, length us, event | category | flops | bytes accessed | tf_op | source)
XLA Modules:
  0.0 140.9 jit_solution(12192963044529781056)
XLA Ops:
  0.0 139.0 %layer.1 = bf16[128,2048]{1,0:T(8,128)(2,1)} custom-call(bf16[128,2048]{1,0:T(8,128)(2,1)} %bitcast.22, bf16[128,2048]{1,0:T(8,128)(2,1)} %bitcast.23, bf16[128,2048]{1,0:T(8,128)(2,1)} %bitcast.24, f32[1024,128]{1,0:T(8,128)} %constant.4.clone.cos_hbm, f32[1024,128]{1,0:T(8,128)} %constant.5.clone.sin_hbm, f32[2]{0:T(128)} %lambda_ref.1, ...), custom_call_target="tpu_custom_call" | custom-call | tf_op jit(solution)/shard_map/layer/pallas_call | solution.py:647
  139.0 1.9 %copy.19 = bf16[1,128,2048]{2,1,0:T(8,128)(2,1)} copy(bf16[1,128,2048]{2,1,0:T(8,128)(2,1)} %bitcast.21) | data formatting | bytes 1048576

commit v4 on v3

--- a/solution.py
+++ b/solution.py
@@ -132,7 +132,7 @@
     scale = map_dim ** (-0.5)
     capacity = outgoing.shape[1]
     units = gate_w.shape[1]
-    wide = math.gcd(model, 512)
+    wide = math.gcd(model, 1024)
     half = jnp.bfloat16
 
     def peer(k):
@@ -512,7 +512,7 @@
         def _():
             returned[k] = value
 
-    tile = math.gcd(units, 256)
+    tile = math.gcd(units, 512)
     held = 2 * groups * capacity
 
     def expand(k):
@@ -527,13 +527,15 @@
                 up = jnp.dot(value, up_w[:, cols], preferred_element_type=jnp.float32)
                 hidden[:, cols] = (gate / (1.0 + jnp.exp(-gate)) * up).astype(half)
 
+    broad = math.gcd(model, 2048)
+
     def contract(k):
         with scope("ffn_down"):
-            @pl.loop(0, model // wide)
+            @pl.loop(0, model // broad)
             def _(n):
-                cols = tile_of(n, wide)
+                cols = tile_of(n, broad)
                 part = jnp.dot(hidden[...], down_w[:, cols], preferred_element_type=jnp.float32)
-                part = part.astype(half).reshape(2, groups, capacity, wide)
+                part = part.astype(half).reshape(2, groups, capacity, broad)
                 own[k, :, :, cols] = part[0]
                 arrived[k, 1, :, :, cols] = part[1]
 
@@ -643,7 +645,7 @@
     blocks = pltpu.VMEM((heads, count, tokens, lanes), half)
     table = pltpu.VMEM((tokens, lanes), jnp.float32)
     pool_rows = max(out_weight.shape[0], slots * groups)
-    wide = math.gcd(model, 512)
+    wide = math.gcd(model, 1024)
     updated = pl.pallas_call(
         functools.partial(layer_kernel, count, groups),
         out_shape=jax.ShapeDtypeStruct((tokens, model), half),

time: 141 us -> 137 us (0.972)
  Pallas kernels: 139 us -> 135 us
    pallas_call x1, Pallas kernels: 139 us -> 135 us  [local(): pl.pallas_call(functools.partial(layer_kernel, count, groups), out_shape=...]
where the time goes in v4:
time: 137 us
  Pallas kernels  135 us (99%)
  local copies, waits for them, and re-layouts  1.88 us (1%)
    pallas_call x1, Pallas kernels, local(): pl.pallas_call(functools.partial(layer_kernel, count, groups), out_shape=...  135 us

profile of v4, /device:TPU:0, one launch (start us, length us, event | category | flops | bytes accessed | tf_op | source)
XLA Modules:
  0.0 137.0 jit_solution(1167529746650805089)
XLA Ops:
  0.0 135.1 %layer.1 = bf16[128,2048]{1,0:T(8,128)(2,1)} custom-call(bf16[128,2048]{1,0:T(8,128)(2,1)} %bitcast.22, bf16[128,2048]{1,0:T(8,128)(2,1)} %bitcast.23, bf16[128,2048]{1,0:T(8,128)(2,1)} %bitcast.24, f32[1024,128]{1,0:T(8,128)} %constant.4.clone.cos_hbm, f32[1024,128]{1,0:T(8,128)} %constant.5.clone.sin_hbm, f32[2]{0:T(128)} %lambda_ref.1, ...), custom_call_target="tpu_custom_call" | custom-call | tf_op jit(solution)/shard_map/layer/pallas_call | solution.py:649
  135.1 1.9 %copy.19 = bf16[1,128,2048]{2,1,0:T(8,128)(2,1)} copy(bf16[1,128,2048]{2,1,0:T(8,128)(2,1)} %bitcast.21) | data formatting | bytes 1048576
